TPU v7x, 32 devices: a whole 2x2x4 slice. The times are simulated.
32 devices in a mesh: sp: 8 (over z, x), tp: 4 (over y, core).
Axes of the slice: x: 2, y: 2, z: 4, core: 2. Of those that a mesh axis runs over, the one named last changes fastest.
Arguments:
- tokens: bfloat16 [2048, 2048], P('sp', 'tp'), may hold values from -6 to 6
- norm_gain: float32 [2048], replicated, may hold values from 0.1 to 1.9
- query_one: bfloat16 [2048, 512], P('sp', 'tp'), may hold values from -1 to 1
- key_one: bfloat16 [2048, 512], P('sp', 'tp'), may hold values from -1 to 1
- query_two: bfloat16 [2048, 512], P('sp', 'tp'), may hold values from -0.15625 to 0.15625
- key_two: bfloat16 [2048, 512], P('sp', 'tp'), may hold values from -0.15625 to 0.15625
- value_weight: bfloat16 [2048, 1024], P('sp', 'tp'), may hold values from -0.5 to 0.5
- pool_weight: bfloat16 [2048, 1024], P('sp', 'tp'), may hold values from -0.125 to 0.125
- lambda_head: float32 [8], replicated, may hold values from 0.3 to 0.8
- head_gain: float32 [128], replicated, may hold values from 0.1 to 1.9
- group_weight: bfloat16 [8, 128, 128], replicated, may hold values from -0.5 to 0.5
- pool_scale: float32 [1024], replicated, may hold values from 0.1 to 1.9
- out_attn: bfloat16 [1024, 2048], P('tp', 'sp'), may hold values from -0.125 to 0.125
- out_pool: bfloat16 [1024, 2048], P('tp', 'sp'), may hold values from -0.125 to 0.125
Outputs:
- mixed: bfloat16 [2048, 2048], P(('sp', 'tp'))
All inputs are finite; a program needn't handle non-finite values.
Results may differ from a plain program's by a relative error of at most 0.013.
Values may be sent and summed in bfloat16 or wider, within the bound.
A program may use at most 128 MiB of HBM per device.

v0:
```python
import math
import jax
import jax.numpy as jnp
from jax import lax
from jax.sharding import PartitionSpec as P

HEAD_DIM = 64
VALUE_DIM = 128
GROUP_DIM = 128
rope_base = 500000.0
head_scale = 0.8
norm_floor = 1e-06
head_floor = 0.001
masked_score = -1e30
pool_reach = 15
key_block = 1024


def from_behind(x, axis, by):
    peers = lax.axis_size(axis)
    pairs = [(i, i + by) for i in range(peers) if 0 <= i + by < peers]
    return lax.ppermute(x, axis, pairs)


def rotate(values_in, positions):
    half_dim = values_in.shape[-1] // 2
    inverse = rope_base ** (-(jnp.arange(half_dim, dtype=jnp.float32) * 2.0 / values_in.shape[-1]))
    angles = positions.astype(jnp.float32)[:, None] * inverse[None, :]
    cosine = jnp.cos(angles)[:, None, :]
    sine_part = jnp.sin(angles)[:, None, :]
    first_half = values_in[..., :half_dim]
    second_half = values_in[..., half_dim:]
    return jnp.concatenate(
        [
            first_half * cosine - second_half * sine_part,
            second_half * cosine + first_half * sine_part,
        ],
        axis=-1,
    )


def body(
    tokens,
    norm_gain,
    query_one,
    key_one,
    query_two,
    key_two,
    value_weight,
    pool_weight,
    lambda_head,
    head_gain,
    group_weight,
    pool_scale,
    out_attn,
    out_pool,
):
    tok_rows = tokens.shape[0]
    local_heads = query_one.shape[1] // HEAD_DIM
    local_groups = pool_weight.shape[1] // GROUP_DIM
    tp_index = lax.axis_index("tp")
    positions = lax.axis_index("sp") * tok_rows + jnp.arange(tok_rows, dtype=jnp.int32)
    score_scale = HEAD_DIM ** (-0.5)
    gathered = lax.all_gather(tokens, "tp", axis=1, tiled=True)
    float_rows = gathered.astype(jnp.float32)
    normed = (
        float_rows
        * lax.rsqrt(jnp.mean(float_rows * float_rows, axis=-1, keepdims=True) + norm_floor)
        * norm_gain
    ).astype(jnp.bfloat16)

    def contract(shard_part):
        return jnp.dot(normed, shard_part, preferred_element_type=jnp.float32)

    pieces = (
        lax.all_gather(query_one, "sp", axis=0, tiled=True),
        lax.all_gather(key_one, "sp", axis=0, tiled=True),
        lax.all_gather(query_two, "sp", axis=0, tiled=True),
        lax.all_gather(key_two, "sp", axis=0, tiled=True),
        lax.all_gather(value_weight, "sp", axis=0, tiled=True),
    )
    projected = tuple((contract(shard_part) for shard_part in pieces))
    pool_proj = contract(lax.all_gather(pool_weight, "sp", axis=0, tiled=True))

    def turned(flat_part):
        return rotate(flat_part.reshape(tok_rows, local_heads, HEAD_DIM), positions).astype(
            jnp.bfloat16
        )

    query_a = turned(projected[0])
    key_a = turned(projected[1]).reshape(tok_rows, local_heads * HEAD_DIM)
    query_b = turned(projected[2])
    key_b = turned(projected[3]).reshape(tok_rows, local_heads * HEAD_DIM)
    value_rows = projected[4].astype(jnp.bfloat16)
    queries = (query_a, query_b)
    initial = (
        jnp.full((2, tok_rows, local_heads), masked_score, jnp.float32),
        jnp.zeros((2, tok_rows, local_heads), jnp.float32),
        jnp.zeros((2, tok_rows, local_heads, VALUE_DIM), jnp.float32),
    )
    pieces = (
        lax.all_gather(key_a, "sp", axis=0, tiled=True),
        lax.all_gather(key_b, "sp", axis=0, tiled=True),
        lax.all_gather(value_rows, "sp", axis=0, tiled=True),
    )
    key_rows = pieces[0].shape[0]
    key_span = math.gcd(key_rows, key_block)
    count_blocks = key_rows // key_span
    stacked = tuple((member.reshape(count_blocks, key_span, local_heads, -1) for member in pieces))

    def step_block(carried, inputs):
        maxima, totals, accums = carried
        block_a, block_b, block_v, block_id = inputs
        key_pos = block_id * key_span + jnp.arange(key_span, dtype=jnp.int32)
        visible = (key_pos[None, :] <= positions[:, None])[:, None, :]
        new_maxima, new_totals, new_accums = ([], [], [])
        for map_index, key_part in enumerate((block_a, block_b)):
            scores = (
                jnp.einsum(
                    "qhd,khd->qhk", queries[map_index], key_part, preferred_element_type=jnp.float32
                )
                * score_scale
            )
            scores = jnp.where(visible, scores, masked_score)
            top_now = jnp.maximum(maxima[map_index], jnp.max(scores, axis=-1))
            factor = jnp.exp(maxima[map_index] - top_now)
            weights = jnp.where(visible, jnp.exp(scores - top_now[..., None]), 0.0)
            new_maxima.append(top_now)
            new_totals.append(totals[map_index] * factor + jnp.sum(weights, axis=-1))
            product = jnp.einsum(
                "qhk,khd->qhd",
                weights.astype(jnp.bfloat16),
                block_v,
                preferred_element_type=jnp.float32,
            )
            new_accums.append(accums[map_index] * factor[..., None] + product)
        return ((jnp.stack(new_maxima), jnp.stack(new_totals), jnp.stack(new_accums)), None)

    result_state, _ = lax.scan(
        step_block,
        initial,
        (stacked[0], stacked[1], stacked[2], jnp.arange(count_blocks, dtype=jnp.int32)),
    )
    maxima, totals, accums = result_state
    map_means = accums / totals[..., None]
    lambda_local = lax.dynamic_slice_in_dim(lambda_head, tp_index * local_heads, local_heads, 0)
    differed = map_means[0] - lambda_local[None, :, None] * map_means[1]
    scaled = (
        differed
        * lax.rsqrt(jnp.mean(differed * differed, axis=-1, keepdims=True) + head_floor)
        * head_gain
        * head_scale
    )
    attn_out = scaled.reshape(tok_rows, local_heads * VALUE_DIM).astype(jnp.bfloat16)
    pool_rows = pool_proj.astype(jnp.bfloat16)
    prior_rows = from_behind(pool_rows[tok_rows - pool_reach :], "sp", 1)
    extended = jnp.concatenate([prior_rows, pool_rows], axis=0).astype(jnp.float32)
    group_ids = tp_index * local_groups + jnp.arange(local_groups, dtype=jnp.int32)
    windows = jnp.left_shift(2, group_ids % 4)
    channel_windows = (windows[:, None] + jnp.zeros((1, GROUP_DIM), jnp.int32)).reshape(-1)
    window_sum = jnp.zeros((tok_rows, local_groups * GROUP_DIM), jnp.float32)
    for lag_steps in range(pool_reach + 1):
        keep_mask = (lag_steps < channel_windows).astype(jnp.float32)
        window_sum = (
            window_sum
            + extended[pool_reach - lag_steps : pool_reach - lag_steps + tok_rows]
            * keep_mask[None, :]
        )
    counts = jnp.minimum(positions[:, None] + 1, channel_windows[None, :]).astype(jnp.float32)
    window_mean = window_sum / counts - pool_rows.astype(jnp.float32)
    local_mixing = lax.dynamic_slice_in_dim(group_weight, tp_index * local_groups, local_groups, 0)
    grouped = jnp.einsum(
        "tgc,gcd->tgd",
        window_mean.astype(jnp.bfloat16).reshape(tok_rows, local_groups, GROUP_DIM),
        local_mixing,
        preferred_element_type=jnp.float32,
    )
    scale_local = lax.dynamic_slice_in_dim(
        pool_scale, tp_index * local_groups * GROUP_DIM, local_groups * GROUP_DIM, 0
    )
    pooled = (grouped.reshape(tok_rows, local_groups * GROUP_DIM) * scale_local).astype(
        jnp.bfloat16
    )
    attn_cols, pool_cols = (
        lax.all_gather(out_attn, "sp", axis=1, tiled=True),
        lax.all_gather(out_pool, "sp", axis=1, tiled=True),
    )
    return lax.psum_scatter(
        (
            jnp.dot(attn_out, attn_cols, preferred_element_type=jnp.float32)
            + jnp.dot(pooled, pool_cols, preferred_element_type=jnp.float32)
        ).astype(jnp.bfloat16),
        "tp",
        scatter_dimension=0,
        tiled=True,
    )


def solution(mesh):
    in_specs = (
        P("sp", "tp"),
        P(),
        P("sp", "tp"),
        P("sp", "tp"),
        P("sp", "tp"),
        P("sp", "tp"),
        P("sp", "tp"),
        P("sp", "tp"),
        P(),
        P(),
        P(),
        P(),
        P("tp", "sp"),
        P("tp", "sp"),
    )
    out_specs = P(("sp", "tp"), None)
    return jax.shard_map(body, mesh=mesh, in_specs=in_specs, out_specs=out_specs, check_vma=False)
```

profile of v0, /device:TPU:0, one launch (start us, length us, event | category | flops | bytes accessed | tf_op | source)
XLA Modules:
  0.0 335.7 jit_solution(8059476277659263844)
XLA Ops:
  6.5 0.7 all-gather.7.cloned.1.call-update
  7.3 0.7 all-gather.9.cloned.1.call-update
  8.1 0.7 all-gather.15.cloned.1.call-update
  8.8 19.6 %all-gather.7.cloned.1.call-done = bf16[256,2048]{1,0:T(8,128)(2,1)} async-done(((bf16[256,512]{1,0:T(8,128)(2,1)}), bf16[256,2048]{1,0:T(8,128)(2,1)}) %all-gather.7.cloned.1.call-update) | async-done | bytes 1048592 | tf_op jit(solution)/shard_map/all_gather | solution.py:64
  28.4 1.5 fusion.41
  29.9 1.6 fusion.43
  31.5 39.3 %all-gather.9.cloned.1.call-done = bf16[2048,256]{1,0:T(8,128)(2,1)} async-done(((bf16[256,256]{1,0:T(8,128)(2,1)}), bf16[2048,256]{1,0:T(8,128)(2,1)}) %all-gather.9.cloned.1.call-update) | async-done | bytes 1048592 | tf_op jit(solution)/shard_map/all_gather | solution.py:80
  70.8 2.3 convolution_convert_fusion.1
  73.1 0.0 all-gather.13.cloned.1.call-start
  73.2 0.5 all-gather.13.cloned.1.call-update
  73.8 0.5 all-gather.17.cloned.1.call-update
  74.4 0.1 fusion.75
  74.5 0.6 broadcast_bitcast_fusion.1
  75.1 0.5 fusion.91
  75.6 31.9 %all_gather.37 = bf16[2048,128]{1,0:T(8,128)(2,1)S(1)} all-gather(bf16[256,128]{1,0:T(8,128)(2,1)S(1)} %copy-done.4), channel_id=1, replica_groups=mesh['sp'=8,'tp'=4] {'sp'}, dimensions={0}, use_global_device_ids=true | all-gather | bytes 589824 | tf_op jit(solution)/shard_map/all_gather | solution.py:77
  107.5 32.2 %all_gather.39 = bf16[2048,128]{1,0:T(8,128)(2,1)S(1)} all-gather(bf16[256,128]{1,0:T(8,128)(2,1)S(1)} %copy-done.5), channel_id=1, replica_groups=mesh['sp'=8,'tp'=4] {'sp'}, dimensions={0}, use_global_device_ids=true | all-gather | bytes 589824 | tf_op jit(solution)/shard_map/all_gather | solution.py:76
  139.7 32.3 %all_gather.40 = bf16[2048,128]{1,0:T(8,128)(2,1)S(1)} all-gather(bf16[256,128]{1,0:T(8,128)(2,1)S(1)} %copy-done.6), channel_id=1, replica_groups=mesh['sp'=8,'tp'=4] {'sp'}, dimensions={0}, use_global_device_ids=true | all-gather | bytes 589824 | tf_op jit(solution)/shard_map/all_gather | solution.py:79
  172.0 31.9 %all_gather.42 = bf16[2048,128]{1,0:T(8,128)(2,1)S(1)} all-gather(bf16[256,128]{1,0:T(8,128)(2,1)S(1)} %copy-done.7), channel_id=1, replica_groups=mesh['sp'=8,'tp'=4] {'sp'}, dimensions={0}, use_global_device_ids=true | all-gather | bytes 589824 | tf_op jit(solution)/shard_map/all_gather | solution.py:78
  203.9 0.2 multiply_cosine_fusion
  204.1 0.7 dynamic_slice.24
  204.9 0.1 broadcast_bitcast_fusion
  204.9 0.8 dynamic_slice.26
  205.7 0.5 fusion.97
  206.2 0.5 fusion.98
  206.7 0.5 fusion.99
  207.2 0.5 fusion.100
  207.7 0.1 subtract_convert_fusion
  207.8 32.2 %all_gather.41 = bf16[2048,128]{0,1:T(8,128)(2,1)S(1)} all-gather(bf16[256,128]{0,1:T(8,128)(2,1)S(1)} %bitcast.251), channel_id=1, replica_groups=mesh['sp'=8,'tp'=4] {'sp'}, dimensions={0}, use_global_device_ids=true | all-gather | bytes 589824 | tf_op jit(solution)/shard_map/all_gather | solution.py:103
  240.0 31.2 %all_gather.38 = bf16[2048,128]{0,1:T(8,128)(2,1)S(1)} all-gather(bf16[256,128]{0,1:T(8,128)(2,1)S(1)} %bitcast.252), channel_id=1, replica_groups=mesh['sp'=8,'tp'=4] {'sp'}, dimensions={0}, use_global_device_ids=true | all-gather | bytes 589824 | tf_op jit(solution)/shard_map/all_gather | solution.py:102
  271.1 1.7 convolution_convert_fusion
  272.8 1.5 collective-permute-start
  274.3 0.4 reshape.311
  274.7 0.9 copy.23
  275.6 0.4 reshape.308
  276.0 0.1 copy.22
  276.2 0.7 fusion.70
  277.0 0.1 fusion.61
  277.1 1.3 reshape.313
  278.5 18.7 %while.15 = (s32[]{:T(128)}, f32[2,256,2]{1,2,0:T(2,128)S(1)}, f32[2,256,2]{1,2,0:T(2,128)S(1)}, f32[2,256,2,128]{1,3,2,0:T(8,128)S(1)}, s32[2]{0:T(128)S(1)}, /...) while((s32[]{:T(128)}, f32[2,256,2]{1,2,0:T(2,128)S(1)}, ...), condition=%wide.region_6.7_spmd.clone, body=%wide.region_1.6_spmd.clone.sunk | while | flops 416947456 | bytes 34822424 | solution.py:139
  278.6 0.7 dynamic_slice.53
  279.9 0.2 broadcast_compare_fusion.2
  280.1 1.8 fusion.141
  282.0 0.4 constant_dynamic-slice_fusion.2
  282.4 0.4 copy.37
  282.8 2.4 fusion.147
  285.2 1.0 fusion.143
  286.2 0.6 fusion.146
  286.9 0.6 fusion.145
  287.5 0.4 copy-done.3
  287.9 0.7 dynamic_slice.53
  289.2 0.2 broadcast_compare_fusion.2
  289.5 1.8 fusion.141
  291.3 0.4 constant_dynamic-slice_fusion.2
  291.7 0.4 copy.37
  292.1 2.4 fusion.147
  294.5 1.0 fusion.143
  295.5 0.6 fusion.146
  296.2 0.6 fusion.145
  296.9 0.4 copy-done.3
  297.3 0.1 fusion.67
  297.5 0.1 fusion.64
  297.6 1.7 fusion.101
  299.4 2.7 fusion.40
  302.1 26.7 %reduce-scatter.2.cloned.1.call-done = bf16[64,2048]{1,0:T(8,128)(2,1)} async-done(((bf16[256,2048]{1,0:T(8,128)(2,1)}), bf16[64,2048]{1,0:T(8,128)(2,1)}) %reduce-scatter.2.cloned.1.call-update) | async-done | bytes 262160 | tf_op jit(solution)/shard_map/reduce_scatter | solution.py:188
  (73 shorter events, 0.8 us)
Async XLA Ops:
  6.5 269.7 %copy-start = (bf16[8,128,128]{2,1,0:T(8,128)(2,1)S(1)}, bf16[8,128,128]{2,1,0:T(8,128)(2,1)}, u32[]{:S(2)}) copy-start(bf16[8,128,128]{2,1,0:T(8,128)(2,1)} %param.26) | copy-start | bytes 786436
  6.5 21.8 %all-gather.7.cloned.1.call-start = ((), (), s32[]{:S(2)}) async-start(), calls=%async_computation.1 | async-start | bytes 1310720 | tf_op jit(solution)/shard_map/all_gather | solution.py:64
  7.3 63.5 %all-gather.9.cloned.1.call-start = ((), (), s32[]{:S(2)}) async-start(), calls=%async_computation.2 | async-start | bytes 1179648 | tf_op jit(solution)/shard_map/all_gather | solution.py:80
  8.0 263.1 %all-gather.15.cloned.1.call-start = ((), (), s32[]{:S(2)}) async-start(), calls=%async_computation.5 | async-start | bytes 1179648 | tf_op jit(solution)/shard_map/all_gather | solution.py:83
  8.7 268.4 %all-gather.11.cloned.1.call-start = ((), (), s32[]{:S(2)}) async-start(), calls=%async_computation.3 | async-start | bytes 1179648 | tf_op jit(solution)/shard_map/all_gather | solution.py:104
  29.9 45.7 %copy-start.4 = (bf16[256,128]{1,0:T(8,128)(2,1)S(1)}, bf16[256,128]{1,0:T(8,128)(2,1)}, u32[]{:S(2)}) copy-start(bf16[256,128]{1,0:T(8,128)(2,1)} %param.19) | copy-start | bytes 196612
  31.5 76.1 %copy-start.5 = (bf16[256,128]{1,0:T(8,128)(2,1)S(1)}, bf16[256,128]{1,0:T(8,128)(2,1)}, u32[]{:S(2)}) copy-start(bf16[256,128]{1,0:T(8,128)(2,1)} %param.18) | copy-start | bytes 196612
  31.5 108.2 %copy-start.6 = (bf16[256,128]{1,0:T(8,128)(2,1)S(1)}, bf16[256,128]{1,0:T(8,128)(2,1)}, u32[]{:S(2)}) copy-start(bf16[256,128]{1,0:T(8,128)(2,1)} %param.21) | copy-start | bytes 196612
  31.5 140.5 %copy-start.7 = (bf16[256,128]{1,0:T(8,128)(2,1)S(1)}, bf16[256,128]{1,0:T(8,128)(2,1)}, u32[]{:S(2)}) copy-start(bf16[256,128]{1,0:T(8,128)(2,1)} %param.20) | copy-start | bytes 196612
  31.5 173.4 %copy-start.8 = (f32[128]{0:T(128)S(1)}, f32[128]{0:T(128)}, u32[]{:S(2)}) copy-start(f32[128]{0:T(128)} %param.25) | copy-start | bytes 1540
  73.1 224.5 %all-gather.13.cloned.1.call-start = ((), (), s32[]{:S(2)}) async-start(), calls=%async_computation.4 | async-start | bytes 1179648 | tf_op jit(solution)/shard_map/all_gather | solution.py:185
  73.7 225.6 %all-gather.17.cloned.1.call-start = ((), (), s32[]{:S(2)}) async-start(), calls=%async_computation.6 | async-start | bytes 1179648 | tf_op jit(solution)/shard_map/all_gather | solution.py:186
  74.3 254.5 %reduce-scatter.2.cloned.1.call-start = ((), (), s32[]{:S(2)}) async-start(), calls=%async_computation.7 | async-start | bytes 1310720 | tf_op jit(solution)/shard_map/reduce_scatter | solution.py:188
  272.8 3.3 collective-permute-start
  274.3 1.9 copy-start.10
  274.3 1.9 copy-start.11
  278.5 3.4 %copy-start.2 = (bf16[2,1024,2,64]{1,3,2,0:T(8,128)(2,1)}, bf16[2,1024,2,64]{1,3,2,0:T(8,128)(2,1)S(1)}, u32[]{:S(2)}) copy-start(bf16[2,1024,2,64]{1,3,2,0:T(8,128)(2,1)S(1)} %get-tuple-element.317) | copy-start | bytes 1572868 | tf_op jit(solution)/shard_map/while
  282.8 2.4 copy-start.1
  282.8 2.4 copy-start.9
  286.9 1.0 copy-start.3
  287.9 3.4 %copy-start.2 = (bf16[2,1024,2,64]{1,3,2,0:T(8,128)(2,1)}, bf16[2,1024,2,64]{1,3,2,0:T(8,128)(2,1)S(1)}, u32[]{:S(2)}) copy-start(bf16[2,1024,2,64]{1,3,2,0:T(8,128)(2,1)S(1)} %get-tuple-element.317) | copy-start | bytes 1572868 | tf_op jit(solution)/shard_map/while
  292.1 2.4 copy-start.1
  292.1 2.4 copy-start.9
  296.2 1.0 copy-start.3
Sparse Core Ops, SparseCore 0:
  8.9 19.4 all-gather.6
  30.5 40.2 all-gather.8
  72.9 41.6 all-gather.14
  116.6 41.4 all-gather.10
  160.0 42.5 all-gather.12
  204.4 40.6 all-gather.16
  302.2 26.5 reduce-scatter.1
where the time goes:
time: 336 us
  blocking collectives  192 us (57%)
  waiting for transfers between devices  88.8 us (26%)
  matrix products  22.8 us (7%)
  between operations  13.8 us (4%)
  local copies, waits for them, and re-layouts  9.14 us (3%)
  other arithmetic  6.18 us (2%)
    all_gather x1, waiting for transfers between devices, body(): lax.all_gather(value_weight, 'sp', axis=0, tiled=True)  39.3 us
    all_gather x1, blocking collectives, body(): lax.all_gather(key_two, 'sp', axis=0, tiled=True)  32.3 us
    all_gather x1, blocking collectives, body(): lax.all_gather(key_b, 'sp', axis=0, tiled=True)  32.2 us
    all_gather x1, blocking collectives, body(): lax.all_gather(query_one, 'sp', axis=0, tiled=True)  32.2 us
    all_gather x1, blocking collectives, body(): lax.all_gather(query_two, 'sp', axis=0, tiled=True)  31.9 us
    all_gather x1, blocking collectives, body(): lax.all_gather(key_one, 'sp', axis=0, tiled=True)  31.9 us
    all_gather x1, blocking collectives, body(): lax.all_gather(key_a, 'sp', axis=0, tiled=True)  31.2 us
    reduce_scatter x1, waiting for transfers between devices, body(): lax.psum_scatter((jnp.dot(attn_out, attn_cols, preferred_element_type=jnp...  26.7 us
  transfers between devices with their start and end apart: 8, of which 3 were waited for; matrix products, arithmetic and copies ran while one was open for 10% of the time, Pallas kernels for 0%

commit v1 on v0

--- a/solution.py
+++ b/solution.py
@@ -61,7 +61,7 @@
     tp_index = lax.axis_index("tp")
     positions = lax.axis_index("sp") * tok_rows + jnp.arange(tok_rows, dtype=jnp.int32)
     score_scale = HEAD_DIM ** (-0.5)
-    gathered = lax.all_gather(tokens, "tp", axis=1, tiled=True)
+    gathered = jnp.concatenate(jax.lax.all_gather(tokens, "tp"), 1)
     float_rows = gathered.astype(jnp.float32)
     normed = (
         float_rows

time: 336 us -> 342 us (1.018)
  local copies, waits for them, and re-layouts: 9.14 us -> 16.1 us
  waiting for transfers between devices: 88.8 us -> 82.9 us
    all_gather x1, waiting for transfers between devices: 39.3 us -> 34.3 us  [body(): lax.all_gather(value_weight, 'sp', axis=0, tiled=True)]
    dot_general x0 -> x4, local copies, waits for them, and re-layouts: none -> 4.05 us  [contract(): return jnp.dot(normed, shard_part, preferred_element_type=jnp.float32)]
  transfers between devices with their start and end apart: 8 -> 8, of which waited for: 3 -> 3; matrix products, arithmetic and copies ran while one was open for 10% -> 13% of each run, Pallas kernels for 0% -> 0%
where the time goes in v1:
time: 342 us; the launch traced here: 341 us
  blocking collectives  191 us (56%)
  waiting for transfers between devices  82.9 us (24%)
  matrix products  24.3 us (7%)
  local copies, waits for them, and re-layouts  16.1 us (5%)
  between operations  13.9 us (4%)
  other arithmetic  9.06 us (3%)
    all_gather x1, waiting for transfers between devices, body(): lax.all_gather(value_weight, 'sp', axis=0, tiled=True)  34.3 us
    all_gather x1, blocking collectives, body(): lax.all_gather(key_two, 'sp', axis=0, tiled=True)  32.4 us
    all_gather x1, blocking collectives, body(): lax.all_gather(key_b, 'sp', axis=0, tiled=True)  32.2 us
    all_gather x1, blocking collectives, body(): lax.all_gather(query_two, 'sp', axis=0, tiled=True)  32 us
    all_gather x1, blocking collectives, body(): lax.all_gather(query_one, 'sp', axis=0, tiled=True)  31.8 us
    all_gather x1, blocking collectives, body(): lax.all_gather(key_one, 'sp', axis=0, tiled=True)  31.7 us
    all_gather x1, blocking collectives, body(): lax.all_gather(key_a, 'sp', axis=0, tiled=True)  31.2 us
    reduce_scatter x1, waiting for transfers between devices, body(): lax.psum_scatter((jnp.dot(attn_out, attn_cols, preferred_element_type=jnp...  25.8 us
  transfers between devices with their start and end apart: 8, of which 3 were waited for; matrix products, arithmetic and copies ran while one was open for 13% of the time, Pallas kernels for 0%

profile of v1, /device:TPU:0, one launch (start us, length us, event | category | flops | bytes accessed | tf_op | source)
XLA Modules:
  0.0 340.9 jit_solution(18240347365860580711)
XLA Ops:
  6.5 0.7 all-gather.18.cloned.1.call-update
  7.3 0.7 all-gather.8.cloned.1.call-update
  8.1 0.7 all-gather.14.cloned.1.call-update
  8.8 19.6 %all-gather.18.cloned.1.call-done = bf16[1024,512]{1,0:T(8,128)(2,1)} async-done(((bf16[256,512]{1,0:T(8,128)(2,1)}), bf16[1024,512]{1,0:T(8,128)(2,1)}) %all-gather.18.cloned.1.call-update) | async-done | bytes 1048592 | tf_op jit(solution)/shard_map/all_gather | solution.py:64
  28.4 2.8 convert_bitcast_fusion
  31.2 3.0 copy.63
  34.2 0.3 fusion.41
  34.5 1.9 fusion.45
  36.5 34.3 %all-gather.8.cloned.1.call-done = bf16[2048,256]{1,0:T(8,128)(2,1)} async-done(((bf16[256,256]{1,0:T(8,128)(2,1)}), bf16[2048,256]{1,0:T(8,128)(2,1)}) %all-gather.8.cloned.1.call-update) | async-done | bytes 1048592 | tf_op jit(solution)/shard_map/all_gather | solution.py:80
  70.8 2.4 convolution_convert_fusion.1
  73.2 0.5 all-gather.12.cloned.1.call-update
  73.8 0.5 all-gather.16.cloned.1.call-update
  74.4 0.7 fusion.78
  75.1 0.6 broadcast_bitcast_fusion.1
  75.7 0.5 fusion.94
  76.3 31.7 %all_gather.41 = bf16[2048,128]{1,0:T(8,128)(2,1)S(1)} all-gather(bf16[256,128]{1,0:T(8,128)(2,1)S(1)} %copy-done.7), channel_id=1, replica_groups=mesh['sp'=8,'tp'=4] {'sp'}, dimensions={0}, use_global_device_ids=true | all-gather | bytes 589824 | tf_op jit(solution)/shard_map/all_gather | solution.py:77
  108.0 1.0 copy.55
  109.0 31.8 %all_gather.43 = bf16[2048,128]{1,0:T(8,128)(2,1)S(1)} all-gather(bf16[256,128]{1,0:T(8,128)(2,1)S(1)} %copy-done.8), channel_id=1, replica_groups=mesh['sp'=8,'tp'=4] {'sp'}, dimensions={0}, use_global_device_ids=true | all-gather | bytes 589824 | tf_op jit(solution)/shard_map/all_gather | solution.py:76
  140.8 1.0 copy.57
  141.8 32.4 %all_gather.44 = bf16[2048,128]{1,0:T(8,128)(2,1)S(1)} all-gather(bf16[256,128]{1,0:T(8,128)(2,1)S(1)} %copy-done.9), channel_id=1, replica_groups=mesh['sp'=8,'tp'=4] {'sp'}, dimensions={0}, use_global_device_ids=true | all-gather | bytes 589824 | tf_op jit(solution)/shard_map/all_gather | solution.py:79
  174.2 1.0 copy.59
  175.2 32.0 %all_gather.46 = bf16[2048,128]{1,0:T(8,128)(2,1)S(1)} all-gather(bf16[256,128]{1,0:T(8,128)(2,1)S(1)} %copy-done.10), channel_id=1, replica_groups=mesh['sp'=8,'tp'=4] {'sp'}, dimensions={0}, use_global_device_ids=true | all-gather | bytes 589824 | tf_op jit(solution)/shard_map/all_gather | solution.py:78
  207.3 1.0 copy.61
  208.3 0.2 multiply_cosine_fusion
  208.6 0.8 dynamic_slice.26
  209.4 0.3 fusion.46
  209.7 0.5 copy.54
  210.3 1.4 fusion.100
  211.7 1.4 fusion.101
  213.1 0.3 fusion.102
  213.4 0.3 fusion.103
  213.8 32.2 %all_gather.45 = bf16[2048,128]{0,1:T(8,128)(2,1)S(1)} all-gather(bf16[256,128]{0,1:T(8,128)(2,1)S(1)} %bitcast.284), channel_id=1, replica_groups=mesh['sp'=8,'tp'=4] {'sp'}, dimensions={0}, use_global_device_ids=true | all-gather | bytes 589824 | tf_op jit(solution)/shard_map/all_gather | solution.py:103
  246.0 31.2 %all_gather.42 = bf16[2048,128]{0,1:T(8,128)(2,1)S(1)} all-gather(bf16[256,128]{0,1:T(8,128)(2,1)S(1)} %bitcast.285), channel_id=1, replica_groups=mesh['sp'=8,'tp'=4] {'sp'}, dimensions={0}, use_global_device_ids=true | all-gather | bytes 589824 | tf_op jit(solution)/shard_map/all_gather | solution.py:102
  277.2 1.7 convolution_convert_fusion
  278.9 1.5 collective-permute-start
  280.5 0.4 reshape.349
  280.9 0.9 copy.65
  281.8 0.4 reshape.348
  282.4 0.7 fusion.73
  283.3 1.3 reshape.350
  284.7 18.7 %while.15 = (s32[]{:T(128)}, f32[2,256,2]{1,2,0:T(2,128)S(1)}, f32[2,256,2]{1,2,0:T(2,128)S(1)}, f32[2,256,2,128]{1,3,2,0:T(8,128)S(1)}, s32[2]{0:T(128)S(1)}, /...) while((s32[]{:T(128)}, f32[2,256,2]{1,2,0:T(2,128)S(1)}, ...), condition=%wide.region_6.7_spmd.clone, body=%wide.region_1.6_spmd.clone.sunk | while | flops 416947456 | bytes 34822424 | solution.py:139
  284.8 0.7 dynamic_slice.53
  286.1 0.2 broadcast_compare_fusion.2
  286.3 1.9 fusion.144
  288.2 0.4 constant_dynamic-slice_fusion.2
  288.6 0.4 copy.87
  289.0 2.4 fusion.150
  291.4 1.0 fusion.146
  292.4 0.6 fusion.149
  293.1 0.6 fusion.148
  293.7 0.4 copy-done.6
  294.1 0.7 dynamic_slice.53
  295.5 0.2 broadcast_compare_fusion.2
  295.7 1.9 fusion.144
  297.6 0.4 constant_dynamic-slice_fusion.2
  297.9 0.4 copy.87
  298.4 2.4 fusion.150
  300.8 1.0 fusion.146
  301.8 0.6 fusion.149
  302.5 0.6 fusion.148
  303.1 0.4 copy-done.6
  303.9 1.7 fusion.104
  305.6 2.7 fusion.40
  308.3 25.8 %reduce-scatter.2.cloned.1.call-done = bf16[64,2048]{1,0:T(8,128)(2,1)} async-done(((bf16[256,2048]{1,0:T(8,128)(2,1)}), bf16[64,2048]{1,0:T(8,128)(2,1)}) %reduce-scatter.2.cloned.1.call-update) | async-done | bytes 262160 | tf_op jit(solution)/shard_map/reduce_scatter | solution.py:188
  (98 shorter events, 1.5 us)
Async XLA Ops:
  6.5 275.8 %copy-start = (bf16[8,128,128]{2,1,0:T(8,128)(2,1)S(1)}, bf16[8,128,128]{2,1,0:T(8,128)(2,1)}, u32[]{:S(2)}) copy-start(bf16[8,128,128]{2,1,0:T(8,128)(2,1)} %param.26) | copy-start | bytes 786436
  6.5 21.8 %all-gather.18.cloned.1.call-start = ((), (), s32[]{:S(2)}) async-start(), calls=%async_computation.7 | async-start | bytes 1310720 | tf_op jit(solution)/shard_map/all_gather | solution.py:64
  7.3 63.5 %all-gather.8.cloned.1.call-start = ((), (), s32[]{:S(2)}) async-start(), calls=%async_computation.1 | async-start | bytes 1179648 | tf_op jit(solution)/shard_map/all_gather | solution.py:80
  8.0 269.2 %all-gather.14.cloned.1.call-start = ((), (), s32[]{:S(2)}) async-start(), calls=%async_computation.4 | async-start | bytes 1179648 | tf_op jit(solution)/shard_map/all_gather | solution.py:83
  8.7 274.6 %all-gather.10.cloned.1.call-start = ((), (), s32[]{:S(2)}) async-start(), calls=%async_computation.2 | async-start | bytes 1179648 | tf_op jit(solution)/shard_map/all_gather | solution.py:104
  31.2 3.0 copy-start.1
  31.2 3.3 copy-start.11
  36.4 39.8 %copy-start.7 = (bf16[256,128]{1,0:T(8,128)(2,1)S(1)}, bf16[256,128]{1,0:T(8,128)(2,1)}, u32[]{:S(2)}) copy-start(bf16[256,128]{1,0:T(8,128)(2,1)} %param.19) | copy-start | bytes 196612
  36.5 72.6 %copy-start.8 = (bf16[256,128]{1,0:T(8,128)(2,1)S(1)}, bf16[256,128]{1,0:T(8,128)(2,1)}, u32[]{:S(2)}) copy-start(bf16[256,128]{1,0:T(8,128)(2,1)} %param.18) | copy-start | bytes 196612
  73.1 68.7 %copy-start.9 = (bf16[256,128]{1,0:T(8,128)(2,1)S(1)}, bf16[256,128]{1,0:T(8,128)(2,1)}, u32[]{:S(2)}) copy-start(bf16[256,128]{1,0:T(8,128)(2,1)} %param.21) | copy-start | bytes 196612
  73.2 230.7 %all-gather.12.cloned.1.call-start = ((), (), s32[]{:S(2)}) async-start(), calls=%async_computation.3 | async-start | bytes 1179648 | tf_op jit(solution)/shard_map/all_gather | solution.py:185
  73.8 231.8 %all-gather.16.cloned.1.call-start = ((), (), s32[]{:S(2)}) async-start(), calls=%async_computation.5 | async-start | bytes 1179648 | tf_op jit(solution)/shard_map/all_gather | solution.py:186
  74.3 259.7 %reduce-scatter.2.cloned.1.call-start = ((), (), s32[]{:S(2)}) async-start(), calls=%async_computation.6 | async-start | bytes 1310720 | tf_op jit(solution)/shard_map/reduce_scatter | solution.py:188
  108.0 67.2 %copy-start.10 = (bf16[256,128]{1,0:T(8,128)(2,1)S(1)}, bf16[256,128]{1,0:T(8,128)(2,1)}, u32[]{:S(2)}) copy-start(bf16[256,128]{1,0:T(8,128)(2,1)} %param.20) | copy-start | bytes 196612
  140.8 67.7 %copy-start.16 = (f32[8]{0:T(128)S(1)}, f32[8]{0:T(128)}, u32[]{:S(2)}) copy-start(f32[8]{0:T(128)} %param.24) | copy-start | bytes 100
  140.8 67.8 %copy-start.15 = (f32[128]{0:T(128)S(1)}, f32[128]{0:T(128)}, u32[]{:S(2)}) copy-start(f32[128]{0:T(128)} %param.25) | copy-start | bytes 1540
  210.2 2.9 copy-start.2
  211.7 1.7 copy-start.3
  278.9 3.4 collective-permute-start
  280.4 1.9 copy-start.12
  280.4 1.9 copy-start.13
  280.5 1.9 copy-start.14
  280.5 1.9 copy-start.18
  280.5 1.9 copy-start.19
  284.7 3.5 %copy-start.5 = (bf16[2,1024,2,64]{1,3,2,0:T(8,128)(2,1)}, bf16[2,1024,2,64]{1,3,2,0:T(8,128)(2,1)S(1)}, u32[]{:S(2)}) copy-start(bf16[2,1024,2,64]{1,3,2,0:T(8,128)(2,1)S(1)} %get-tuple-element.339) | copy-start | bytes 1572868 | tf_op jit(solution)/shard_map/while
  289.0 2.4 copy-start.4
  289.0 2.4 copy-start.17
  293.1 1.0 copy-start.6
  294.1 3.4 %copy-start.5 = (bf16[2,1024,2,64]{1,3,2,0:T(8,128)(2,1)}, bf16[2,1024,2,64]{1,3,2,0:T(8,128)(2,1)S(1)}, u32[]{:S(2)}) copy-start(bf16[2,1024,2,64]{1,3,2,0:T(8,128)(2,1)S(1)} %get-tuple-element.339) | copy-start | bytes 1572868 | tf_op jit(solution)/shard_map/while
  298.4 2.4 copy-start.4
  298.4 2.4 copy-start.17
  302.4 1.0 copy-start.6
Sparse Core Ops, SparseCore 0:
  8.9 19.4 all-gather.17
  30.5 40.2 all-gather.7
  72.9 41.2 all-gather.13
  116.2 42.0 all-gather.9
  160.2 41.5 all-gather.11
  203.7 41.5 all-gather.15
  308.4 25.6 reduce-scatter.1
